TPU v7x, 512 devices: a whole 4x4x16 slice. The times are simulated.
512 devices in a mesh: fs: 64 (over z, y), tp: 8 (over x, core).
Axes of the slice: x: 4, y: 4, z: 16, core: 2. Of those that a mesh axis runs over, the one named last changes fastest.
Arguments:
- tokens: bfloat16 [16384, 2048], P('fs', 'tp'), may hold values from -16 to 16, as said below
- mix_gain: bfloat16 [2048], P('tp'), may hold values from 0.099609375 to 1.8984375
- query_weight: bfloat16 [2048, 512], P('fs', 'tp'), may hold values from -0.125 to 0.125
- key_weight: bfloat16 [2048, 512], P('fs', 'tp'), may hold values from -0.125 to 0.125
- value_weight: bfloat16 [2048, 1024], P('fs', 'tp'), may hold values from -0.125 to 0.125
- output_gate_weight: bfloat16 [2048, 1024], P('fs', 'tp'), may hold values from -0.125 to 0.125
- out_weight: bfloat16 [1024, 2048], P('tp', 'fs'), may hold values from -0.1875 to 0.1875
- head_rates: float32 [8], P('tp'), may hold values from 0 to 1, as said below
- block_scale: float32 [128], P('fs'), may hold values from 0.5 to 2
- ffn_gain: bfloat16 [2048], P('tp'), may hold values from 0.099609375 to 1.8984375
- ff_gate: bfloat16 [2048, 5632], P('fs', 'tp'), may hold values from -0.125 to 0.125
- ff_up: bfloat16 [2048, 5632], P('fs', 'tp'), may hold values from -0.125 to 0.125
- ff_down: bfloat16 [5632, 2048], P('tp', 'fs'), may hold values from -0.078125 to 0.078125
- final_gain: bfloat16 [2048], P('tp'), may hold values from 0.099609375 to 1.8984375
Outputs:
- layer_out: bfloat16 [16384, 2048], P('fs', 'tp')
Inputs may be any that keep to these rules, and one draw needn't show every extreme that they name: `tokens`: column blocks of the activations have different scales. `head_rates`: positive rates.
All inputs are finite; a program needn't handle non-finite values.
Results may differ from a plain program's by a relative error of at most 0.014.
Values may be sent and summed in bfloat16 or wider, within the bound.
A program may use at most 64 MiB of HBM per device.

v0:
```python
import jax
import jax.numpy as jnp
from jax import lax
from jax.sharding import Mesh
from jax.sharding import PartitionSpec as P

D = 2048
DK = 64
DV = 128
BLK = 128
SEQ_LEN = 256
FS = ("fs_0", "fs_1")
EPS = 1e-06
THETA = 10000.0


def gather_turned(arrays, axis, dims):
    turned = [jnp.moveaxis(a, dim, 0) for a, dim in zip(arrays, dims)]
    both = jnp.concatenate([t.reshape(len(t), -1) for t in turned], axis=1)
    filled, at, outs = (lax.all_gather(both, axis, axis=0, tiled=True), 0, [])
    for t, dim in zip(turned, dims):
        share = filled[:, at : at + t[0].size].reshape(-1, *t.shape[1:])
        outs.append(jnp.moveaxis(share, 0, dim))
        at += t[0].size
    return tuple(outs)


def sent_together(arrays, axis, dim, along):
    widths = [a.shape[along] for a in arrays]
    both = jnp.concatenate(arrays, axis=along)
    filled = lax.all_gather(both, axis, axis=dim, tiled=True)
    return tuple(jnp.split(filled, [sum(widths[:k]) for k in range(1, len(widths))], axis=along))


def laid_out(tiles, dim):
    lengths = list(tiles.shape[1:])
    lengths[dim] *= tiles.shape[0]
    return jnp.moveaxis(tiles, 0, dim).reshape(lengths)


def copy_for_each(shard, axis):
    size = lax.axis_size(axis)
    return lax.all_to_all(
        jnp.broadcast_to(shard[None], (size, *shard.shape)), axis, 0, 0, tiled=True
    )


def gather_directly(shard, axis, dim):
    return laid_out(copy_for_each(shard, axis), dim)


def gathered_by_axis(shard, axes, dim):
    filled = shard
    for number in range(len(axes) - 1, -1, -1):
        filled = lax.all_gather(filled, axes[number], axis=dim, tiled=True)
    return filled


def in_blocks(shard, dim, size):
    lengths = shard.shape
    tiles = shard.reshape(*lengths[:dim], size, lengths[dim] // size, *lengths[dim + 1 :])
    return jnp.moveaxis(tiles, dim, 0)


def sent_and_summed(shard, axis, dim):
    size = lax.axis_size(axis)
    tiles = lax.all_to_all(in_blocks(shard, dim, size), axis, 0, 0, tiled=True)
    return jnp.sum(tiles.astype(jnp.float32), axis=0)


def of_everyone(shard, axis):
    return copy_for_each(shard, axis).sum(axis=0)


def rms_norm(values, gain):
    scale = lax.rsqrt(jnp.mean(values * values, axis=-1, keepdims=True) + EPS)
    return values * scale * gain.astype(jnp.float32)


def rotate(values, positions):
    half = values.shape[-1] // 2
    inverse = THETA ** (-jnp.arange(half, dtype=jnp.float32) / half)
    angle = positions.astype(jnp.float32)[:, None] * inverse
    cosine = jnp.cos(angle)[:, None, :]
    sine = jnp.sin(angle)[:, None, :]
    first = values[..., :half]
    second = values[..., half:]
    return jnp.concatenate(
        [first * cosine - second * sine, second * cosine + first * sine], axis=-1
    )


def retain(query, key, value, rates, scales):
    rows, heads_here, width_k = query.shape
    width_v = value.shape[-1]
    nblk = rows // BLK
    hi = lax.Precision.HIGHEST
    qblk = query.astype(jnp.float32).reshape(nblk, BLK, heads_here, width_k)
    kblk = key.astype(jnp.float32).reshape(nblk, BLK, heads_here, width_k)
    vblk = value.astype(jnp.float32).reshape(nblk, BLK, heads_here, width_v)
    logdec = -rates[None, :] * scales[:, None]
    steps = jnp.arange(BLK, dtype=jnp.float32)
    offset = steps[:, None] - steps[None, :]
    causal = offset >= 0
    inside = jnp.where(
        causal[None, None],
        jnp.exp(logdec[:, :, None, None] * jnp.where(causal, offset, 0.0)[None, None]),
        0.0,
    )
    scores = jnp.einsum("nchd,nmhd->nhcm", qblk, kblk, precision=hi) * inside
    inner = jnp.einsum("nhcm,nmhe->nche", scores, vblk, precision=hi)
    zeta = jnp.exp(logdec[:, :, None] * (BLK - 1.0 - steps)[None, None, :])
    kv_block = jnp.einsum(
        "nchd,nche->nhde", kblk * jnp.transpose(zeta, (0, 2, 1))[..., None], vblk, precision=hi
    )
    hold = jnp.exp(logdec * BLK)
    per_seq = SEQ_LEN // BLK
    fresh = (jnp.arange(nblk, dtype=jnp.int32) % per_seq == 0).astype(jnp.float32)

    def advance(state, inputs):
        kv_now, hold_now, fresh_now = inputs
        before = state * (1.0 - fresh_now)
        return (before * hold_now[:, None, None] + kv_now, before)

    start = jnp.zeros((heads_here, width_k, width_v), jnp.float32)
    _, before = lax.scan(advance, start, (kv_block, hold, fresh))
    xi = jnp.exp(logdec[:, :, None] * (steps + 1.0)[None, None, :])
    cross = jnp.einsum(
        "nchd,nhde->nche", qblk * jnp.transpose(xi, (0, 2, 1))[..., None], before, precision=hi
    )
    total = inner + cross
    total = total * lax.rsqrt(jnp.mean(total * total, axis=-1, keepdims=True) + EPS)
    return total.reshape(rows, heads_here * width_v)


def body(
    tokens,
    mix_gain,
    query_weight,
    key_weight,
    value_weight,
    output_gate_weight,
    out_weight,
    head_rates,
    block_scale,
    ffn_gain,
    ff_gate,
    ff_up,
    ff_down,
    final_gain,
):
    rows = tokens.shape[0]
    heads_here = head_rates.shape[0]
    groups = lax.axis_size("tp")
    positions = jnp.arange(rows, dtype=jnp.int32) % SEQ_LEN
    whole, gain_whole = gather_turned((tokens, mix_gain), "tp", (1, 0))
    normed = rms_norm(whole.astype(jnp.float32), gain_whole).astype(jnp.bfloat16)
    collected = sent_together(
        (query_weight, key_weight, value_weight, output_gate_weight), FS, 0, 1
    )
    qproj, kproj, vproj, gproj = tuple(
        (jnp.dot(normed, weight, preferred_element_type=jnp.float32) for weight in collected)
    )
    query = rotate(qproj.reshape(rows, heads_here, DK), positions).astype(jnp.bfloat16)
    key = (rotate(kproj.reshape(rows, heads_here, DK), positions) * DK ** (-0.5)).astype(
        jnp.bfloat16
    )
    value = vproj.astype(jnp.bfloat16).reshape(rows, heads_here, DV)
    normret = retain(query, key, value, head_rates, block_scale)
    gated = (normret * jax.nn.silu(gproj)).astype(jnp.bfloat16)
    all_heads = gather_directly(gated, "tp", 1)
    head_rows = gathered_by_axis(out_weight, FS, 1)
    feature_block = lax.all_to_all(head_rows, "tp", split_axis=1, concat_axis=0, tiled=True)
    width = all_heads.shape[1] // groups
    left = all_heads.reshape(rows, groups, width)
    right = feature_block.reshape(groups, width, feature_block.shape[1])
    partial_sums = jnp.einsum(
        "rng,nge->nre", left, right, preferred_element_type=jnp.float32
    ).astype(jnp.bfloat16)
    mix = jnp.sum(partial_sums.astype(jnp.float32), axis=0)
    resid = (tokens.astype(jnp.float32) + mix).astype(jnp.bfloat16)
    whole2, gain2 = gather_turned((resid, ffn_gain), "tp", (1, 0))
    normed2 = rms_norm(whole2.astype(jnp.float32), gain2).astype(jnp.bfloat16)
    gate_rows, up_rows = sent_together((ff_gate, ff_up), FS, 0, 1)
    gate_part = jnp.dot(normed2, gate_rows, preferred_element_type=jnp.float32)
    up_part = jnp.dot(normed2, up_rows, preferred_element_type=jnp.float32)
    hidden = (jax.nn.silu(gate_part) * up_part).astype(jnp.bfloat16)
    down_terms = jnp.dot(
        hidden, gathered_by_axis(ff_down, FS, 1), preferred_element_type=jnp.float32
    )
    ffn = sent_and_summed(down_terms.astype(jnp.bfloat16), "tp", 1)
    total = resid.astype(jnp.float32) + ffn
    squares = of_everyone(jnp.sum(total * total, axis=-1, keepdims=True), "tp")
    scale = lax.rsqrt(squares / D + EPS)
    return (total * scale * final_gain.astype(jnp.float32)).astype(jnp.bfloat16)


def solution(mesh):
    finer = Mesh(mesh.devices.reshape(16, 4, mesh.shape["tp"]), ("fs_0", "fs_1", "tp"))
    return jax.shard_map(
        body,
        mesh=finer,
        in_specs=(
            P(FS, "tp"),
            P("tp"),
            P(FS, "tp"),
            P(FS, "tp"),
            P(FS, "tp"),
            P(FS, "tp"),
            P("tp", FS),
            P("tp"),
            P(FS),
            P("tp"),
            P(FS, "tp"),
            P(FS, "tp"),
            P("tp", FS),
            P("tp"),
        ),
        out_specs=P(FS, "tp"),
        check_vma=False,
    )
```

profile of v0, /device:TPU:1, one launch (start us, length us, event | category | flops | bytes accessed | tf_op | source)
XLA Modules:
  0.0 515.7 jit_solution(17452584656318330392)
XLA Ops:
  6.5 0.7 reshape.400
  7.2 1.6 pad_maximum_fusion
  8.9 1.4 pad_maximum_fusion.3
  10.3 10.6 %all_gather.26 = bf16[128,128]{0,1:T(8,128)(2,1)S(1)} all-gather(bf16[128,32]{0,1:T(8,128)(2,1)} %param.22), channel_id=1, replica_groups=mesh['fs_0'=16,'fs_1'=4,'tp'=8] {'fs_1'}, dimensions={1}, use_global_device_ids=true | all-gather | bytes 40960 | tf_op jit(solution)/shard_map/all_gather | solution.py:55
  20.9 31.9 %all_gather.27 = bf16[128,2048]{0,1:T(8,128)(2,1)S(1)} all-gather(bf16[128,128]{0,1:T(8,128)(2,1)S(1)} %all_gather.26), channel_id=1, replica_groups=mesh['fs_0'=16,'fs_1'=4,'tp'=8] {'fs_0'}, dimensions={1}, use_global_device_ids=true | all-gather | bytes 557056 | tf_op jit(solution)/shard_map/all_gather | solution.py:55
  52.8 1.0 copy.31
  53.8 14.1 %all-to-all-start.1 = ((bf16[128,8,256]{2,0,1:T(8,128)(2,1)}), bf16[128,8,256]{2,0,1:T(8,128)(2,1)S(1)}, u32[]{:S(2)}, u32[]{:S(2)}) async-start(bf16[128,8,256]{2,0,1:T(8,128)(2,1)} %copy.31), calls=%async_computation.1 | async-start | bytes 1048576 | tf_op jit(solution)/shard_map/all_to_all | solution.py:173
  68.9 1.6 fusion.4
  70.5 0.8 slice_convert_fusion.1
  71.2 109.0 %all-gather.8.cloned.1.call-done = bf16[2048,384]{1,0:T(8,128)(2,1)} async-done(((bf16[32,384]{1,0:T(8,128)(2,1)}), bf16[2048,384]{1,0:T(8,128)(2,1)}) %all-gather.8.cloned.1.call-update) | async-done | bytes 1572880 | tf_op jit(solution)/shard_map/all_gather | solution.py:31
  180.3 2.0 convolution_bitcast_fusion
  182.3 1.6 convolution_bitcast_fusion.1
  184.2 1.5 convolution_convert_fusion.2
  185.9 5.0 while.13
  192.1 1.6 fusion.35
  193.7 0.9 broadcast_in_dim.29
  194.6 15.1 %all-to-all-start = ((bf16[8,256,128]{2,1,0:T(8,128)(2,1)}), bf16[8,256,128]{2,1,0:T(8,128)(2,1)S(1)}, u32[]{:S(2)}, u32[]{:S(2)}) async-start(bf16[8,256,128]{2,1,0:T(8,128)(2,1)} %broadcast_in_dim.29), calls=%async_computation | async-start | bytes 1048576 | tf_op jit(solution)/shard_map/all_to_all | solution.py:43
  209.7 9.3 %all-to-all-done = bf16[8,256,128]{2,1,0:T(8,128)(2,1)S(1)} async-done(((bf16[8,256,128]{2,1,0:T(8,128)(2,1)}), bf16[8,256,128]{2,1,0:T(8,128)(2,1)S(1)}, u32[]{:S(2)}, u32[]{:S(2)}) %all-to-all-start) | async-done | bytes 524320 | tf_op jit(solution)/shard_map/all_to_all | solution.py:43
  219.5 0.7 pad_maximum_fusion.1
  220.3 0.7 pad_maximum_fusion.2
  221.1 10.0 %all_gather.30 = bf16[704,128]{0,1:T(8,128)(2,1)} all-gather(bf16[704,32]{0,1:T(8,128)(2,1)S(1)} %copy-done.5), channel_id=1, replica_groups=mesh['fs_0'=16,'fs_1'=4,'tp'=8] {'fs_1'}, dimensions={1}, use_global_device_ids=true | all-gather | bytes 225280 | tf_op jit(solution)/shard_map/all_gather | solution.py:55
  231.1 15.0 %all-gather.10.cloned.1.call-done = bf16[2048,257]{0,1:T(8,128)(2,1)} async-done(((bf16[256,257]{0,1:T(8,128)(2,1)}), bf16[2048,257]{0,1:T(8,128)(2,1)}) %all-gather.10.cloned.1.call-update) | async-done | bytes 1052688 | tf_op jit(solution)/shard_map/all_gather | solution.py:20
  246.0 1.5 fusion.7
  247.6 0.8 slice_convert_fusion
  248.3 142.7 %all-gather.12.cloned.1.call-done = bf16[2048,1408]{1,0:T(8,128)(2,1)} async-done(((bf16[32,1408]{1,0:T(8,128)(2,1)}), bf16[2048,1408]{1,0:T(8,128)(2,1)}) %all-gather.12.cloned.1.call-update) | async-done | bytes 5767184 | tf_op jit(solution)/shard_map/all_gather | solution.py:31
  391.0 3.7 fusion.2
  394.7 68.0 %all-gather.14.cloned.1.call-done = bf16[704,2048]{0,1:T(8,128)(2,1)} async-done(((bf16[704,128]{0,1:T(8,128)(2,1)}), bf16[704,2048]{0,1:T(8,128)(2,1)}) %all-gather.14.cloned.1.call-update) | async-done | bytes 2883600 | tf_op jit(solution)/shard_map/all_gather | solution.py:55
  462.7 7.2 %convolution_convert_fusion = bf16[256,2048]{1,0:T(8,128)(2,1)S(1)} fusion(bf16[704,2048]{0,1:T(8,128)(2,1)} %all-gather.14.cloned.1.call-done, bf16[2048,1408]{1,0:T(8,128)(2,1)} %all-gather.12.cloned.1.call-done, f32[256,704]{0,1:T(8,128)S(1)} %fusion.2, f32[2048]{0:T(1024)S(1)} %bitcast.82, f32[256]{0:T(256)S(1)} %add_rsqrt_fusion.1, ...), kind=kOutput, calls=%fused_computation.12 | convolution fusion | flops 1480097792 | bytes 9118720 | tf_op jit(solution)/shard_map/dot_general | solution.py:188
  470.1 28.6 %all_to_all.31 = bf16[8,256,256]{2,1,0:T(8,128)(2,1)S(1)} all-to-all(bf16[8,256,256]{2,1,0:T(8,128)(2,1)S(1)} %bitcast.70), channel_id=1, replica_groups=mesh['fs_0'=16,'fs_1'=4,'tp'=8] {'tp'}, dimensions={0} | all-to-all | bytes 2097152 | tf_op jit(solution)/shard_map/all_to_all | solution.py:67
  499.5 4.3 all-to-all-start.3
  503.8 4.6 all-to-all-done.3
  508.4 0.8 multiply_convert_fusion
  (75 shorter events, 7.1 us)
Async XLA Ops:
  6.5 62.2 %copy-start.6 = (f32[2]{0:T(128)S(1)}, f32[2]{0:T(128)}, u32[]{:S(2)}) copy-start(f32[2]{0:T(128)} %param.24) | copy-start | bytes 28
  6.5 62.3 %all-gather.6.cloned.1.call-start = ((), (), s32[]{:S(2)}) async-start(), calls=%async_computation.4 | async-start | bytes 1216512 | tf_op jit(solution)/shard_map/all_gather | solution.py:20
  8.8 171.5 %all-gather.8.cloned.1.call-start = ((), (), s32[]{:S(2)}) async-start(), calls=%async_computation.5 | async-start | bytes 1597440 | tf_op jit(solution)/shard_map/all_gather | solution.py:31
  53.8 139.9 %all-to-all-start.1 = ((bf16[128,8,256]{2,0,1:T(8,128)(2,1)}), bf16[128,8,256]{2,0,1:T(8,128)(2,1)S(1)}, u32[]{:S(2)}, u32[]{:S(2)}) async-start(bf16[128,8,256]{2,0,1:T(8,128)(2,1)} %copy.31), calls=%async_computation.1 | async-start | bytes 1048576 | tf_op jit(solution)/shard_map/all_to_all | solution.py:173
  68.9 113.5 %copy-start = (bf16[2048,257]{0,1:T(8,128)(2,1)S(1)}, bf16[2048,257]{0,1:T(8,128)(2,1)}, u32[]{:S(2)}) copy-start(bf16[2048,257]{0,1:T(8,128)(2,1)} %all-gather.6.cloned.1.call-done) | copy-start | bytes 3158020
  192.1 17.6 %copy-start.7 = (bf16[256]{0:T(256)(128)(2,1)S(1)}, bf16[256]{0:T(256)(128)(2,1)}, u32[]{:S(2)}) copy-start(bf16[256]{0:T(256)(128)(2,1)} %param.25) | copy-start | bytes 1540
  193.7 25.8 %copy-start.2 = (bf16[256,256]{1,0:T(8,128)(2,1)S(1)}, bf16[256,256]{1,0:T(8,128)(2,1)}, u32[]{:S(2)}) copy-start(bf16[256,256]{1,0:T(8,128)(2,1)} %param.16) | copy-start | bytes 393220
  193.7 26.6 %copy-start.3 = (bf16[32,704]{1,0:T(8,128)(2,1)S(1)}, bf16[32,704]{1,0:T(8,128)(2,1)}, u32[]{:S(2)}) copy-start(bf16[32,704]{1,0:T(8,128)(2,1)} %param.27) | copy-start | bytes 135172
  193.7 26.6 %copy-start.4 = (bf16[32,704]{1,0:T(8,128)(2,1)S(1)}, bf16[32,704]{1,0:T(8,128)(2,1)}, u32[]{:S(2)}) copy-start(bf16[32,704]{1,0:T(8,128)(2,1)} %param.26) | copy-start | bytes 135172
  193.7 27.3 %copy-start.5 = (bf16[704,32]{0,1:T(8,128)(2,1)S(1)}, bf16[704,32]{0,1:T(8,128)(2,1)}, u32[]{:S(2)}) copy-start(bf16[704,32]{0,1:T(8,128)(2,1)} %param.28) | copy-start | bytes 135172
  194.6 24.4 %all-to-all-start = ((bf16[8,256,128]{2,1,0:T(8,128)(2,1)}), bf16[8,256,128]{2,1,0:T(8,128)(2,1)S(1)}, u32[]{:S(2)}, u32[]{:S(2)}) async-start(bf16[8,256,128]{2,1,0:T(8,128)(2,1)} %broadcast_in_dim.29), calls=%async_computation | async-start | bytes 1048576 | tf_op jit(solution)/shard_map/all_to_all | solution.py:43
  209.7 36.4 %all-gather.10.cloned.1.call-start = ((), (), s32[]{:S(2)}) async-start(), calls=%async_computation.6 | async-start | bytes 1216512 | tf_op jit(solution)/shard_map/all_gather | solution.py:20
  220.2 170.8 %all-gather.12.cloned.1.call-start = ((), (), s32[]{:S(2)}) async-start(), calls=%async_computation.7 | async-start | bytes 5857280 | tf_op jit(solution)/shard_map/all_gather | solution.py:31
  221.0 241.7 %all-gather.14.cloned.1.call-start = ((), (), s32[]{:S(2)}) async-start(), calls=%async_computation.8 | async-start | bytes 3342336 | tf_op jit(solution)/shard_map/all_gather | solution.py:55
  391.0 71.7 %copy-start.1 = (bf16[2048,257]{0,1:T(8,128)(2,1)S(1)}, bf16[2048,257]{0,1:T(8,128)(2,1)}, u32[]{:S(2)}) copy-start(bf16[2048,257]{0,1:T(8,128)(2,1)} %all-gather.10.cloned.1.call-done) | copy-start | bytes 3158020
  470.0 33.7 %copy-start.8 = (bf16[256]{0:T(256)(128)(2,1)S(1)}, bf16[256]{0:T(256)(128)(2,1)}, u32[]{:S(2)}) copy-start(bf16[256]{0:T(256)(128)(2,1)} %param.29) | copy-start | bytes 1540
  499.5 8.9 %all-to-all-start.3 = ((f32[8,256,1]{1,2,0:T(1,128)}), f32[8,256,1]{1,2,0:T(1,128)S(1)}, u32[]{:S(2)}, u32[]{:S(2)}) async-start(f32[8,256,1]{1,2,0:T(1,128)} %broadcast_in_dim.30), calls=%async_computation.3 | async-start | bytes 16384 | tf_op jit(solution)/shard_map/all_to_all | solution.py:43
Sparse Core Ops, SparseCore 0:
  9.4 36.6 all-gather.5
  49.1 131.1 all-gather.7
  220.3 25.6 all-gather.9
  248.8 142.1 all-gather.11
  392.9 69.7 all-gather.13
where the time goes:
time: 517 us; the launch traced here: 516 us
  waiting for transfers between devices  349 us (68%)
  blocking collectives  81 us (16%)
  starting transfers between devices  33.6 us (6%)
  matrix products  19.1 us (4%)
  between operations  14.1 us (3%)
  other arithmetic  12 us (2%)
  local copies, waits for them, and re-layouts  5.72 us (1%)
    all_gather x2, waiting for transfers between devices, sent_together(): filled = lax.all_gather(both, axis, axis=dim, tiled=True)  252 us
    all_gather x1, waiting for transfers between devices, gathered_by_axis(): filled = lax.all_gather(filled, axes[number], axis=dim, tiled=True)  68 us
    all_gather x3, blocking collectives, gathered_by_axis(): filled = lax.all_gather(filled, axes[number], axis=dim, tiled=True)  52.5 us
    all_to_all x1, blocking collectives, sent_and_summed(): tiles = lax.all_to_all(in_blocks(shard, dim, size), axis, 0, 0, tiled=True)  28.6 us
    all_to_all x2, starting transfers between devices, copy_for_each(): lax.all_to_all(jnp.broadcast_to(shard[None], (size, *shard.shape)), axis,...  19.4 us
    all_gather x2, waiting for transfers between devices, gather_turned(): filled, at, outs = (lax.all_gather(both, axis, axis=0, tiled=True), 0, [])  15 us
    all_to_all x1, starting transfers between devices, body(): lax.all_to_all(head_rows, 'tp', split_axis=1, concat_axis=0, tiled=True)  14.1 us
    all_to_all x2, waiting for transfers between devices, copy_for_each(): lax.all_to_all(jnp.broadcast_to(shard[None], (size, *shard.shape)), axis,...  14 us
  transfers between devices with their start and end apart: 8, of which 6 were waited for; matrix products, arithmetic and copies ran while one was open for 5% of the time, Pallas kernels for 0%

commit v1 on v0

--- a/solution.py
+++ b/solution.py
@@ -17,7 +17,20 @@
 def gather_turned(arrays, axis, dims):
     turned = [jnp.moveaxis(a, dim, 0) for a, dim in zip(arrays, dims)]
     both = jnp.concatenate([t.reshape(len(t), -1) for t in turned], axis=1)
-    filled, at, outs = (lax.all_gather(both, axis, axis=0, tiled=True), 0, [])
+
+    def bind_series_in(target):
+        b_now = jnp.concatenate(
+            lax.all_to_all(
+                jnp.stack([target for _ in range(lax.psum(1, axis_name=axis))], 0),
+                axis_name=axis,
+                split_axis=0,
+                concat_axis=0,
+            ),
+            0,
+        )
+        return b_now
+
+    filled, at, outs = (bind_series_in(both), 0, [])
     for t, dim in zip(turned, dims):
         share = filled[:, at : at + t[0].size].reshape(-1, *t.shape[1:])
         outs.append(jnp.moveaxis(share, 0, dim))

time: 517 us -> 422 us (0.82)
  waiting for transfers between devices: 349 us -> 231 us
  blocking collectives: 81 us -> 96.1 us
  starting transfers between devices: 33.6 us -> 45.3 us
    all_gather x2, waiting for transfers between devices: 252 us -> 148 us  [sent_together(): filled = lax.all_gather(both, axis, axis=dim, tiled=True)]
    all_to_all x0 -> x1, blocking collectives: none -> 19.1 us  [bind_series_in(): lax.all_to_all(jnp.stack([target for _ in range(lax.psum(1, axis_name=axi...]
    all_gather x2 -> x0, waiting for transfers between devices: 15 us -> none  [gather_turned(): filled, at, outs = (lax.all_gather(both, axis, axis=0, tiled=True), 0, [])]
    all_to_all x0 -> x1, starting transfers between devices: none -> 10.4 us  [bind_series_in(): lax.all_to_all(jnp.stack([target for _ in range(lax.psum(1, axis_name=axi...]
  transfers between devices with their start and end apart: 8 -> 7, of which waited for: 6 -> 5; matrix products, arithmetic and copies ran while one was open for 5% -> 6% of each run, Pallas kernels for 0% -> 0%
where the time goes in v1:
time: 422 us; the launch traced here: 421 us
  waiting for transfers between devices  231 us (55%)
  blocking collectives  96.1 us (23%)
  starting transfers between devices  45.3 us (11%)
  matrix products  18.4 us (4%)
  between operations  14.1 us (3%)
  local copies, waits for them, and re-layouts  8.04 us (2%)
  other arithmetic  7.25 us (2%)
    all_gather x2, waiting for transfers between devices, sent_together(): filled = lax.all_gather(both, axis, axis=dim, tiled=True)  148 us
    all_gather x1, waiting for transfers between devices, gathered_by_axis(): filled = lax.all_gather(filled, axes[number], axis=dim, tiled=True)  68.6 us
    all_gather x3, blocking collectives, gathered_by_axis(): filled = lax.all_gather(filled, axes[number], axis=dim, tiled=True)  48.4 us
    all_to_all x1, blocking collectives, sent_and_summed(): tiles = lax.all_to_all(in_blocks(shard, dim, size), axis, 0, 0, tiled=True)  28.6 us
    all_to_all x2, starting transfers between devices, copy_for_each(): lax.all_to_all(jnp.broadcast_to(shard[None], (size, *shard.shape)), axis,...  19.4 us
    all_to_all x1, blocking collectives, bind_series_in(): lax.all_to_all(jnp.stack([target for _ in range(lax.psum(1, axis_name=axi...  19.1 us
    all_to_all x1, starting transfers between devices, body(): lax.all_to_all(head_rows, 'tp', split_axis=1, concat_axis=0, tiled=True)  15.5 us
    all_to_all x2, waiting for transfers between devices, copy_for_each(): lax.all_to_all(jnp.broadcast_to(shard[None], (size, *shard.shape)), axis,...  14 us
  transfers between devices with their start and end apart: 7, of which 5 were waited for; matrix products, arithmetic and copies ran while one was open for 6% of the time, Pallas kernels for 0%

profile of v1, /device:TPU:1, one launch (start us, length us, event | category | flops | bytes accessed | tf_op | source)
XLA Modules:
  0.0 421.4 jit_solution(10230742687199989510)
XLA Ops:
  6.5 1.4 pad_maximum_fusion.3
  8.1 1.5 pad_maximum_fusion.2
  9.6 0.7 reshape.410
  10.3 0.9 pad_maximum_fusion
  11.2 1.1 stack.4
  12.3 10.4 %all-to-all-start = ((bf16[8,256,257]{1,2,0:T(8,128)(2,1)}), bf16[8,256,257]{1,2,0:T(8,128)(2,1)S(1)}, u32[]{:S(2)}, u32[]{:S(2)}) async-start(bf16[8,256,257]{1,2,0:T(8,128)(2,1)} %stack.4), calls=%async_computation | async-start | bytes 2162688 | tf_op jit(solution)/shard_map/all_to_all | solution.py:23
  22.7 10.5 %all_gather.22 = bf16[704,128]{0,1:T(8,128)(2,1)} all-gather(bf16[704,32]{0,1:T(8,128)(2,1)S(1)} %copy-done.1), channel_id=1, replica_groups=mesh['fs_0'=16,'fs_1'=4,'tp'=8] {'fs_1'}, dimensions={1}, use_global_device_ids=true | all-gather | bytes 225280 | tf_op jit(solution)/shard_map/all_gather | solution.py:68
  33.3 9.8 %all_gather.19 = bf16[128,128]{0,1:T(8,128)(2,1)S(1)} all-gather(bf16[128,32]{0,1:T(8,128)(2,1)S(1)} %copy-done.2), channel_id=1, replica_groups=mesh['fs_0'=16,'fs_1'=4,'tp'=8] {'fs_1'}, dimensions={1}, use_global_device_ids=true | all-gather | bytes 40960 | tf_op jit(solution)/shard_map/all_gather | solution.py:68
  43.1 28.1 %all_gather.20 = bf16[128,2048]{0,1:T(8,128)(2,1)S(1)} all-gather(bf16[128,128]{0,1:T(8,128)(2,1)S(1)} %all_gather.19), channel_id=1, replica_groups=mesh['fs_0'=16,'fs_1'=4,'tp'=8] {'fs_0'}, dimensions={1}, use_global_device_ids=true | all-gather | bytes 557056 | tf_op jit(solution)/shard_map/all_gather | solution.py:68
  71.8 1.0 copy.41
  73.0 15.5 %all-to-all-start.2 = ((bf16[128,8,256]{2,0,1:T(8,128)(2,1)}), bf16[128,8,256]{2,0,1:T(8,128)(2,1)S(1)}, u32[]{:S(2)}, u32[]{:S(2)}) async-start(bf16[128,8,256]{2,0,1:T(8,128)(2,1)} %copy.41), calls=%async_computation.2 | async-start | bytes 1048576 | tf_op jit(solution)/shard_map/all_to_all | solution.py:186
  89.4 56.7 %all-gather.4.cloned.1.call-done = bf16[2048,384]{1,0:T(8,128)(2,1)} async-done(((bf16[32,384]{1,0:T(8,128)(2,1)}), bf16[2048,384]{1,0:T(8,128)(2,1)}) %all-gather.4.cloned.1.call-update) | async-done | bytes 1572880 | tf_op jit(solution)/shard_map/all_gather | solution.py:44
  146.1 1.6 convolution_bitcast_fusion.1
  147.7 1.7 convolution_bitcast_fusion
  149.8 1.6 convolution_convert_fusion.2
  152.0 4.8 %while.13 = (s32[]{:T(128)}, f32[1,64,128]{2,1,0:T(8,128)S(1)}, f32[2,1,64,128]{3,2,1,0:T(8,128)S(1)}, f32[2]{0:T(128)S(1)}, f32[2,1]{0,1:T(1,128)S(1)}, /*index...) while((s32[]{:T(128)}, f32[1,64,128]{2,1,0:T(8,128)S(1)}, ...), condition=%wide.region_2.3_spmd.clone, body=%wide.region_1.2_spmd.clone.sunk | while | flops 49156 | bytes 164000 | solution.py:139
  152.0 0.6 dynamic_slice.22
  154.4 0.6 dynamic_slice.22
  157.4 1.6 fusion.35
  159.0 0.9 broadcast_in_dim.29
  159.9 15.1 %all-to-all-start.1 = ((bf16[8,256,128]{2,1,0:T(8,128)(2,1)}), bf16[8,256,128]{2,1,0:T(8,128)(2,1)S(1)}, u32[]{:S(2)}, u32[]{:S(2)}) async-start(bf16[8,256,128]{2,1,0:T(8,128)(2,1)} %broadcast_in_dim.29), calls=%async_computation.1 | async-start | bytes 1048576 | tf_op jit(solution)/shard_map/all_to_all | solution.py:56
  175.0 9.3 %all-to-all-done.1 = bf16[8,256,128]{2,1,0:T(8,128)(2,1)S(1)} async-done(((bf16[8,256,128]{2,1,0:T(8,128)(2,1)}), bf16[8,256,128]{2,1,0:T(8,128)(2,1)S(1)}, u32[]{:S(2)}, u32[]{:S(2)}) %all-to-all-start.1) | async-done | bytes 524320 | tf_op jit(solution)/shard_map/all_to_all | solution.py:56
  184.9 19.1 %all_to_all.41 = bf16[8,256,257]{1,2,0:T(8,128)(2,1)S(1)} all-to-all(bf16[8,256,257]{1,2,0:T(8,128)(2,1)S(1)} %stack.5), channel_id=1, replica_groups=mesh['fs_0'=16,'fs_1'=4,'tp'=8] {'tp'}, dimensions={0} | all-to-all | bytes 2105344 | tf_op jit(solution)/shard_map/all_to_all | solution.py:23
  204.9 91.6 %all-gather.6.cloned.1.call-done = bf16[2048,1408]{1,0:T(8,128)(2,1)} async-done(((bf16[32,1408]{1,0:T(8,128)(2,1)}), bf16[2048,1408]{1,0:T(8,128)(2,1)}) %all-gather.6.cloned.1.call-update) | async-done | bytes 5767184 | tf_op jit(solution)/shard_map/all_gather | solution.py:44
  296.5 3.3 fusion.2
  299.8 68.6 %all-gather.8.cloned.1.call-done = bf16[704,2048]{0,1:T(8,128)(2,1)} async-done(((bf16[704,128]{0,1:T(8,128)(2,1)}), bf16[704,2048]{0,1:T(8,128)(2,1)}) %all-gather.8.cloned.1.call-update) | async-done | bytes 2883600 | tf_op jit(solution)/shard_map/all_gather | solution.py:68
  368.4 7.2 %convolution_convert_fusion = bf16[256,2048]{1,0:T(8,128)(2,1)S(1)} fusion(bf16[704,2048]{0,1:T(8,128)(2,1)} %all-gather.8.cloned.1.call-done, bf16[2048,1408]{1,0:T(8,128)(2,1)} %all-gather.6.cloned.1.call-done, f32[256,704]{0,1:T(8,128)S(1)} %fusion.2, f32[2048]{0:T(1024)S(1)} %bitcast.110, f32[256]{0:T(256)S(1)} %add_rsqrt_fusion.1, ...), kind=kOutput, calls=%fused_computation.12 | convolution fusion | flops 1480097792 | bytes 9118720 | tf_op jit(solution)/shard_map/dot_general | solution.py:201
  375.7 28.6 %all_to_all.42 = bf16[8,256,256]{2,1,0:T(8,128)(2,1)S(1)} all-to-all(bf16[8,256,256]{2,1,0:T(8,128)(2,1)S(1)} %bitcast.98), channel_id=1, replica_groups=mesh['fs_0'=16,'fs_1'=4,'tp'=8] {'tp'}, dimensions={0} | all-to-all | bytes 2097152 | tf_op jit(solution)/shard_map/all_to_all | solution.py:80
  404.5 0.6 broadcast_in_dim.30
  405.1 4.3 %all-to-all-start.5 = ((f32[8,256,1]{1,2,0:T(1,128)}), f32[8,256,1]{1,2,0:T(1,128)S(1)}, u32[]{:S(2)}, u32[]{:S(2)}) async-start(f32[8,256,1]{1,2,0:T(1,128)} %broadcast_in_dim.30), calls=%async_computation.5 | async-start | bytes 16384 | tf_op jit(solution)/shard_map/all_to_all | solution.py:56
  409.4 4.6 %all-to-all-done.5 = f32[8,256,1]{1,2,0:T(1,128)S(1)} async-done(((f32[8,256,1]{1,2,0:T(1,128)}), f32[8,256,1]{1,2,0:T(1,128)S(1)}, u32[]{:S(2)}, u32[]{:S(2)}) %all-to-all-start.5) | async-done | bytes 8224 | tf_op jit(solution)/shard_map/all_to_all | solution.py:56
  414.1 0.8 multiply_convert_fusion
  (74 shorter events, 6.8 us)
Async XLA Ops:
  6.5 16.2 %copy-start.1 = (bf16[704,32]{0,1:T(8,128)(2,1)S(1)}, bf16[704,32]{0,1:T(8,128)(2,1)}, u32[]{:S(2)}) copy-start(bf16[704,32]{0,1:T(8,128)(2,1)} %param.28) | copy-start | bytes 135172
  6.5 139.6 %all-gather.4.cloned.1.call-start = ((), (), s32[]{:S(2)}) async-start(), calls=%async_computation.6 | async-start | bytes 1597440 | tf_op jit(solution)/shard_map/all_gather | solution.py:44
  8.0 288.5 %all-gather.6.cloned.1.call-start = ((), (), s32[]{:S(2)}) async-start(), calls=%async_computation.7 | async-start | bytes 5857280 | tf_op jit(solution)/shard_map/all_gather | solution.py:44
  9.6 23.7 %copy-start.2 = (bf16[128,32]{0,1:T(8,128)(2,1)S(1)}, bf16[128,32]{0,1:T(8,128)(2,1)}, u32[]{:S(2)}) copy-start(bf16[128,32]{0,1:T(8,128)(2,1)} %param.22) | copy-start | bytes 24580
  12.3 60.7 %copy-start.3 = (f32[2]{0:T(128)S(1)}, f32[2]{0:T(128)}, u32[]{:S(2)}) copy-start(f32[2]{0:T(128)} %param.24) | copy-start | bytes 28
  12.3 60.8 %all-to-all-start = ((bf16[8,256,257]{1,2,0:T(8,128)(2,1)}), bf16[8,256,257]{1,2,0:T(8,128)(2,1)S(1)}, u32[]{:S(2)}, u32[]{:S(2)}) async-start(bf16[8,256,257]{1,2,0:T(8,128)(2,1)} %stack.4), calls=%async_computation | async-start | bytes 2162688 | tf_op jit(solution)/shard_map/all_to_all | solution.py:23
  22.7 345.7 %all-gather.8.cloned.1.call-start = ((), (), s32[]{:S(2)}) async-start(), calls=%async_computation.8 | async-start | bytes 3342336 | tf_op jit(solution)/shard_map/all_gather | solution.py:68
  73.0 86.0 %all-to-all-start.2 = ((bf16[128,8,256]{2,0,1:T(8,128)(2,1)}), bf16[128,8,256]{2,0,1:T(8,128)(2,1)S(1)}, u32[]{:S(2)}, u32[]{:S(2)}) async-start(bf16[128,8,256]{2,0,1:T(8,128)(2,1)} %copy.41), calls=%async_computation.2 | async-start | bytes 1048576 | tf_op jit(solution)/shard_map/all_to_all | solution.py:186
  157.4 17.6 %copy-start.4 = (bf16[256]{0:T(256)(128)(2,1)S(1)}, bf16[256]{0:T(256)(128)(2,1)}, u32[]{:S(2)}) copy-start(bf16[256]{0:T(256)(128)(2,1)} %param.25) | copy-start | bytes 1540
  159.0 25.8 %copy-start = (bf16[256,256]{1,0:T(8,128)(2,1)S(1)}, bf16[256,256]{1,0:T(8,128)(2,1)}, u32[]{:S(2)}) copy-start(bf16[256,256]{1,0:T(8,128)(2,1)} %param.16) | copy-start | bytes 393220
  159.9 24.4 %all-to-all-start.1 = ((bf16[8,256,128]{2,1,0:T(8,128)(2,1)}), bf16[8,256,128]{2,1,0:T(8,128)(2,1)S(1)}, u32[]{:S(2)}, u32[]{:S(2)}) async-start(bf16[8,256,128]{2,1,0:T(8,128)(2,1)} %broadcast_in_dim.29), calls=%async_computation.1 | async-start | bytes 1048576 | tf_op jit(solution)/shard_map/all_to_all | solution.py:56
  375.7 33.7 %copy-start.5 = (bf16[256]{0:T(256)(128)(2,1)S(1)}, bf16[256]{0:T(256)(128)(2,1)}, u32[]{:S(2)}) copy-start(bf16[256]{0:T(256)(128)(2,1)} %param.29) | copy-start | bytes 1540
  405.1 8.9 %all-to-all-start.5 = ((f32[8,256,1]{1,2,0:T(1,128)}), f32[8,256,1]{1,2,0:T(1,128)S(1)}, u32[]{:S(2)}, u32[]{:S(2)}) async-start(f32[8,256,1]{1,2,0:T(1,128)} %broadcast_in_dim.30), calls=%async_computation.5 | async-start | bytes 16384 | tf_op jit(solution)/shard_map/all_to_all | solution.py:56
Sparse Core Ops, SparseCore 0:
  10.3 135.7 all-gather.3
  149.0 147.4 all-gather.5
  298.6 69.7 all-gather.7
